TPU v7x, 32 devices: a whole 2x2x4 slice. The times are simulated.
32 devices in a mesh: grp: 2 (over y), sp: 4 (over z), dp: 4 (over x, core).
Axes of the slice: x: 2, y: 2, z: 4, core: 2. Of those that a mesh axis runs over, the one named last changes fastest.
Arguments:
- activations: bfloat16 [8, 2048, 2048], P(('grp', 'dp'), 'sp'), parts along dimension 0, may hold values from -6 to 6
- value_weight: bfloat16 [2048, 1024], P('sp', 'dp'), may hold values from -0.125 to 0.125
- gate_weight: bfloat16 [2048, 1024], P('sp', 'dp'), may hold values from -0.125 to 0.125
- conv_taps: float32 [31, 1024], replicated, may hold values from -4 to 4
- conv_bias: float32 [1024], replicated, may hold values from -3 to 3
- norm_gain: float32 [1024], replicated, may hold values from 0.1 to 1.9
- norm_bias: float32 [1024], replicated, may hold values from -3 to 3
- out_weight: bfloat16 [1024, 2048], P('sp', 'dp'), may hold values from -0.1875 to 0.1875
Outputs:
- mixed_out: bfloat16 [8, 2048, 2048], P(('grp', 'dp'), 'sp'), parts along dimension 0
There are 2 independent parts, one for each index of `grp`. A program takes and returns all parts, laid end to end along the dimension named above; an argument that names none is the same for every part. Nothing has to cross between parts.
All inputs are finite; a program needn't handle non-finite values.
Results may differ from a plain program's by a relative error of at most 0.013.
Values may be sent and summed in bfloat16 or wider, within the bound.
A program may use at most 64 MiB of HBM per device.

v0:
```python
import jax
import jax.numpy as jnp
from jax import lax
from jax.sharding import PartitionSpec as P

epsilon = 1e-05


def passed_along(value, axis, steps):
    count = lax.axis_size(axis)
    first, last = (max(0, -steps), min(count, count - steps))
    return lax.ppermute(value, axis, [(source, source + steps) for source in range(first, last)])


def local(
    activations, value_weight, gate_weight, conv_taps, conv_bias, norm_gain, norm_bias, out_weight
):
    tokens = activations[0]
    tok_rows = tokens.shape[0]
    kernel_len = conv_taps.shape[0]
    whole_value, whole_gate = (
        lax.all_gather(value_weight, "sp", axis=0, tiled=True),
        lax.all_gather(gate_weight, "sp", axis=0, tiled=True),
    )
    stacked = jnp.stack([whole_value, whole_gate], axis=0)
    both_rows = jnp.einsum(
        "td,kdc->ktc",
        tokens,
        lax.all_gather(stacked, "dp", axis=2, tiled=True),
        preferred_element_type=jnp.float32,
    )
    value_rows = both_rows[0]
    gate_rows = both_rows[1]
    value_half = value_rows.astype(jnp.bfloat16)
    gate_half = gate_rows.astype(jnp.bfloat16)
    gated_rows = (
        value_half.astype(jnp.float32) * jax.nn.sigmoid(gate_half.astype(jnp.float32))
    ).astype(jnp.bfloat16)
    prior = passed_along(gated_rows[tok_rows - (kernel_len - 1) :], "sp", 1)
    padded = jnp.concatenate([prior, gated_rows], axis=0).astype(jnp.float32)
    conv_sum = jnp.zeros(gated_rows.shape, jnp.float32) + conv_bias[None, :]
    for tap_index in range(kernel_len):
        conv_sum = (
            conv_sum + conv_taps[tap_index][None, :] * padded[tap_index : tap_index + tok_rows]
        )
    mean_row = jnp.mean(conv_sum, axis=-1, keepdims=True)
    centered = conv_sum - mean_row
    spread = jnp.mean(centered * centered, axis=-1, keepdims=True)
    normed = centered * lax.rsqrt(spread + epsilon) * norm_gain[None, :] + norm_bias[None, :]
    swished = jax.nn.silu(normed).astype(jnp.bfloat16)
    whole_output = lax.all_gather(out_weight, "sp", axis=0, tiled=True)
    result = jnp.dot(
        swished,
        lax.all_gather(whole_output, "dp", axis=1, tiled=True),
        preferred_element_type=jnp.float32,
    )
    return result.astype(jnp.bfloat16)[None]


def solution(mesh):
    in_specs = (
        P(("grp", "dp"), "sp", None),
        P("sp", "dp"),
        P("sp", "dp"),
        P(),
        P(),
        P(),
        P(),
        P("sp", "dp"),
    )
    out_specs = P(("grp", "dp"), "sp", None)
    return jax.shard_map(local, mesh=mesh, in_specs=in_specs, out_specs=out_specs, check_vma=False)
```

profile of v0, /device:TPU:0, one launch (start us, length us, event | category | flops | bytes accessed | tf_op | source)
XLA Modules:
  0.0 207.2 jit_solution(12494679978274099827)
XLA Ops:
  6.5 0.7 all-gather.6.cloned.1.call-update
  7.3 0.0 all-gather.8.cloned.1.call-start
  7.3 0.7 all-gather.8.cloned.1.call-update
  8.0 0.0 all-gather.12.cloned.1.call-start
  8.1 0.7 all-gather.12.cloned.1.call-update
  8.7 0.0 all-gather.10.cloned.1.call-start
  8.8 30.9 %all-gather.6.cloned.1.call-done = bf16[2048,256]{1,0:T(8,128)(2,1)} async-done(((bf16[512,256]{1,0:T(8,128)(2,1)}), bf16[2048,256]{1,0:T(8,128)(2,1)}) %all-gather.6.cloned.1.call-update) | async-done | bytes 1048592 | tf_op jit(solution)/shard_map/all_gather | solution.py:22
  39.6 29.0 %all-gather.8.cloned.1.call-done = bf16[2048,256]{1,0:T(8,128)(2,1)} async-done(((bf16[512,256]{1,0:T(8,128)(2,1)}), bf16[2048,256]{1,0:T(8,128)(2,1)}) %all-gather.8.cloned.1.call-update) | async-done | bytes 1048592 | tf_op jit(solution)/shard_map/all_gather | solution.py:23
  68.6 3.1 %pad_maximum_fusion = bf16[2,2048,256]{2,1,0:T(8,128)(2,1)} fusion(bf16[1,2048,256]{2,1,0:T(8,128)(2,1)} %bitcast.50, bf16[1,2048,256]{2,1,0:T(8,128)(2,1)} %bitcast.49), kind=kLoop, calls=%fused_computation.64 | loop fusion | flops 1048576 | bytes 4194304 | tf_op jit(solution)/shard_map/stack | solution.py:25
  71.7 0.0 all-gather.10.cloned.1.call-update
  71.7 0.0 all-gather.14.cloned.1.call-start
  71.7 25.8 %all-gather.12.cloned.1.call-done = bf16[1024,512]{1,0:T(8,128)(2,1)} async-done(((bf16[256,512]{1,0:T(8,128)(2,1)}), bf16[1024,512]{1,0:T(8,128)(2,1)}) %all-gather.12.cloned.1.call-update) | async-done | bytes 1048592 | tf_op jit(solution)/shard_map/all_gather | solution.py:51
  97.6 0.0 all-gather.14.cloned.1.call-update
  97.6 0.0 copy-done.2
  97.6 0.1 fusion.44
  97.7 60.0 %all-gather.10.cloned.1.call-done = bf16[2,2048,1024]{2,1,0:T(8,128)(2,1)} async-done(((bf16[2,2048,256]{2,1,0:T(8,128)(2,1)}), bf16[2,2048,1024]{2,1,0:T(8,128)(2,1)}) %all-gather.10.cloned.1.call-update) | async-done | bytes 8388624 | tf_op jit(solution)/shard_map/all_gather | solution.py:29
  157.8 0.0 copy-done
  157.8 8.1 %convert_bitcast_fusion = bf16[2,512,1024]{2,1,0:T(8,128)(2,1)S(1)} fusion(bf16[2,2048,1024]{2,1,0:T(8,128)(2,1)} %all-gather.10.cloned.1.call-done, bf16[1,512,2048]{2,1,0:T(8,128)(2,1)S(1)} %copy-done), kind=kOutput, calls=%fused_computation.68 | convolution fusion | flops 4296015872 | bytes 12582912 | tf_op jit(solution)/shard_map/td,kdc->ktc/dot_general | solution.py:26
  165.8 0.6 multiply_convert_fusion
  166.5 3.4 %collective-permute-start = (bf16[30,1024]{1,0:T(8,128)(2,1)S(1)}, bf16[30,1024]{1,0:T(8,128)(2,1)S(1)}, u32[]{:S(2)}, u32[]{:S(2)}) collective-permute-start(bf16[30,1024]{1,0:T(8,128)(2,1)S(1)} %slice_bitcast_fusion), channel_id=1, source_target_pairs={{0,4},{4,8},{8,12},{1,5},{5,9},{9,13},{2,6},{6,10},{10,14},{3,7},{... | collective-permute-start | bytes 184328 | tf_op jit(solution)/shard_map/ppermute | solution.py:12
  169.9 0.6 fusion.48
  170.5 0.0 copy-start.3
  170.5 1.3 collective-permute-done
  171.8 0.3 maximum_convert_fusion
  172.1 9.8 %fusion.42 = (f32[512]{0:T(512)S(1)}, f32[512,1024]{1,0:T(8,128)S(1)}) fusion(f32[542,1024]{1,0:T(8,128)S(1)} %maximum_convert_fusion, f32[1024]{0:T(1024)S(1)} %bitcast.61, f32[1024]{0:T(1024)S(1)} %bitcast.62, f32[1024]{0:T(1024)S(1)} %bitcast.64, f32[1024]{0:T(1024)S(1)} %bitcast.65, f32[1024]{0:T(1024)S(1)} %bitcast.66, f32[1024]{0:T(1024)S(1)} %bitcast.67, ...), kind=kLoop, calls=%fused_computation.81 | loop fusion | flops 33029632 | bytes 67241984 | tf_op jit(solution)/shard_map/reduce_sum | solution.py:46
  181.9 0.0 copy-start.4
  181.9 0.0 copy-start.5
  182.0 1.3 copy-done.1
  183.3 0.3 multiply_reduce_fusion
  183.6 10.0 %all-gather.14.cloned.1.call-done = bf16[1024,2048]{1,0:T(8,128)(2,1)} async-done(((bf16[1024,512]{1,0:T(8,128)(2,1)}), bf16[1024,2048]{1,0:T(8,128)(2,1)}) %all-gather.14.cloned.1.call-update) | async-done | bytes 4194320 | tf_op jit(solution)/shard_map/all_gather | solution.py:54
  193.7 0.0 copy-done.5
  193.7 7.0 %fusion = bf16[1,512,2048]{2,1,0:T(8,128)(2,1)} fusion(bf16[1024,2048]{1,0:T(8,128)(2,1)} %all-gather.14.cloned.1.call-done, f32[512,1024]{1,0:T(8,128)} %copy-done.1, f32[1024]{0:T(1024)S(1)} %copy-done.4, f32[1024]{0:T(1024)S(1)} %copy-done.5, f32[512]{0:T(512)S(1)} %add_rsqrt_fusion, f32[512]{0:T(512)S(1)} %broadcast_multiply_fusion), kind=kOutput, calls=%fused_computation.1 | convolution fusion | flops 2153250816 | bytes 8400896 | tf_op jit(solution)/shard_map/dot_general | solution.py:52
  (10 shorter events, 0.1 us)
Async XLA Ops:
  6.5 151.2 %copy-start = (bf16[1,512,2048]{2,1,0:T(8,128)(2,1)S(1)}, bf16[1,512,2048]{2,1,0:T(8,128)(2,1)}, u32[]{:S(2)}) copy-start(bf16[1,512,2048]{2,1,0:T(8,128)(2,1)} %param.8) | copy-start | bytes 6291460
  6.5 33.1 %all-gather.6.cloned.1.call-start = ((), (), s32[]{:S(2)}) async-start(), calls=%async_computation | async-start | bytes 1310720 | tf_op jit(solution)/shard_map/all_gather | solution.py:22
  7.3 61.3 %all-gather.8.cloned.1.call-start = ((), (), s32[]{:S(2)}) async-start(), calls=%async_computation.1 | async-start | bytes 1310720 | tf_op jit(solution)/shard_map/all_gather | solution.py:23
  8.0 89.6 %all-gather.12.cloned.1.call-start = ((), (), s32[]{:S(2)}) async-start(), calls=%async_computation.3 | async-start | bytes 1310720 | tf_op jit(solution)/shard_map/all_gather | solution.py:51
  8.7 149.0 %all-gather.10.cloned.1.call-start = ((), (), s32[]{:S(2)}) async-start(), calls=%async_computation.2 | async-start | bytes 10485760 | tf_op jit(solution)/shard_map/all_gather | solution.py:29
  71.7 25.9 %copy-start.2 = (f32[31,1024]{1,0:T(8,128)S(1)}, f32[31,1024]{1,0:T(8,128)}, u32[]{:S(2)}) copy-start(f32[31,1024]{1,0:T(8,128)} %param.11) | copy-start | bytes 380932
  71.7 122.0 %all-gather.14.cloned.1.call-start = ((), (), s32[]{:S(2)}) async-start(), calls=%async_computation.4 | async-start | bytes 5242880 | tf_op jit(solution)/shard_map/all_gather | solution.py:54
  166.5 5.3 %collective-permute-start = (bf16[30,1024]{1,0:T(8,128)(2,1)S(1)}, bf16[30,1024]{1,0:T(8,128)(2,1)S(1)}, u32[]{:S(2)}, u32[]{:S(2)}) collective-permute-start(bf16[30,1024]{1,0:T(8,128)(2,1)S(1)} %slice_bitcast_fusion), channel_id=1, source_target_pairs={{0,4},{4,8},{8,12},{1,5},{5,9},{9,13},{2,6},{6,10},{10,14},{3,7},{... | collective-permute-start | bytes 184328 | tf_op jit(solution)/shard_map/ppermute | solution.py:12
  170.5 1.6 copy-start.3
  181.9 1.3 copy-start.1
  181.9 11.7 %copy-start.4 = (f32[1024]{0:T(1024)S(1)}, f32[1024]{0:T(1024)}, u32[]{:S(2)}) copy-start(f32[1024]{0:T(1024)} %param.14) | copy-start | bytes 12292
  181.9 11.7 %copy-start.5 = (f32[1024]{0:T(1024)S(1)}, f32[1024]{0:T(1024)}, u32[]{:S(2)}) copy-start(f32[1024]{0:T(1024)} %param.13) | copy-start | bytes 12292
Sparse Core Ops, SparseCore 0:
  8.9 30.6 all-gather.5
  41.2 27.3 all-gather.7
  70.2 27.3 all-gather.11
  99.0 58.7 all-gather.9
  159.2 34.4 all-gather.13
where the time goes:
time: 207 us
  waiting for transfers between devices  159 us (77%)
  matrix products  15 us (7%)
  other arithmetic  14.7 us (7%)
  between operations  13.3 us (6%)
  starting transfers between devices  3.55 us (2%)
    all_gather x1, waiting for transfers between devices, local(): lax.all_gather(stacked, 'dp', axis=2, tiled=True)  60 us
    all_gather x1, waiting for transfers between devices, local(): lax.all_gather(value_weight, 'sp', axis=0, tiled=True)  30.9 us
    all_gather x1, waiting for transfers between devices, local(): lax.all_gather(gate_weight, 'sp', axis=0, tiled=True)  29 us
    all_gather x1, waiting for transfers between devices, local(): whole_output = lax.all_gather(out_weight, 'sp', axis=0, tiled=True)  25.8 us
    all_gather x1, waiting for transfers between devices, local(): lax.all_gather(whole_output, 'dp', axis=1, tiled=True)  10 us
    reduce_sum x1, other arithmetic, local(): mean_row = jnp.mean(conv_sum, axis=-1, keepdims=True)  9.83 us
    dot_general x1, matrix products, local(): jnp.einsum('td,kdc->ktc', tokens, lax.all_gather(stacked, 'dp', axis=2, t...  8.06 us
    dot_general x1, matrix products, local(): jnp.dot(swished, lax.all_gather(whole_output, 'dp', axis=1, tiled=True),...  6.96 us
  transfers between devices with their start and end apart: 6, of which 6 were waited for; matrix products, arithmetic and copies ran while one was open for 11% of the time, Pallas kernels for 0%

commit v1 on v0

--- a/solution.py
+++ b/solution.py
@@ -51,7 +51,7 @@
     whole_output = lax.all_gather(out_weight, "sp", axis=0, tiled=True)
     result = jnp.dot(
         swished,
-        lax.all_gather(whole_output, "dp", axis=1, tiled=True),
+        jnp.concatenate(lax.all_gather(whole_output, "dp"), axis=1),
         preferred_element_type=jnp.float32,
     )
     return result.astype(jnp.bfloat16)[None]

time: 207 us -> 229 us (1.11)
  waiting for transfers between devices: 159 us -> 178 us
  local copies, waits for them, and re-layouts: 1.44 us -> 7.62 us
  matrix products: 15 us -> 12.2 us
    all_gather x1, waiting for transfers between devices: 10 us -> 31.2 us  [local(): lax.all_gather(whole_output, 'dp')]
    reshape x0 -> x1, local copies, waits for them, and re-layouts: none -> 6.3 us  [local(): jnp.concatenate(lax.all_gather(whole_output, 'dp'), axis=1)]
    all_gather x1, waiting for transfers between devices: 60 us -> 54.5 us  [local(): lax.all_gather(stacked, 'dp', axis=2, tiled=True)]
    all_gather x1, waiting for transfers between devices: 25.8 us -> 30.9 us  [local(): whole_output = lax.all_gather(out_weight, 'sp', axis=0, tiled=True)]
    dot_general x1, matrix products: 6.96 us -> 4.16 us  [local(): jnp.dot(swished, jnp.concatenate(lax.all_gather(whole_output, 'dp'), axis...]
  transfers between devices with their start and end apart: 6 -> 6, of which waited for: 6 -> 6; matrix products, arithmetic and copies ran while one was open for 11% -> 4% of each run, Pallas kernels for 0% -> 0%
where the time goes in v1:
time: 229 us
  waiting for transfers between devices  178 us (78%)
  other arithmetic  14.6 us (6%)
  between operations  13.3 us (6%)
  matrix products  12.2 us (5%)
  local copies, waits for them, and re-layouts  7.62 us (3%)
  starting transfers between devices  3.55 us (2%)
    all_gather x1, waiting for transfers between devices, local(): lax.all_gather(stacked, 'dp', axis=2, tiled=True)  54.5 us
    all_gather x1, waiting for transfers between devices, local(): lax.all_gather(whole_output, 'dp')  31.2 us
    all_gather x1, waiting for transfers between devices, local(): whole_output = lax.all_gather(out_weight, 'sp', axis=0, tiled=True)  30.9 us
    all_gather x1, waiting for transfers between devices, local(): lax.all_gather(gate_weight, 'sp', axis=0, tiled=True)  29 us
    all_gather x1, waiting for transfers between devices, local(): lax.all_gather(value_weight, 'sp', axis=0, tiled=True)  28.9 us
    reduce_sum x1, other arithmetic, local(): mean_row = jnp.mean(conv_sum, axis=-1, keepdims=True)  9.72 us
    dot_general x1, matrix products, local(): jnp.einsum('td,kdc->ktc', tokens, lax.all_gather(stacked, 'dp', axis=2, t...  8.07 us
    reshape x1, local copies, waits for them, and re-layouts, local(): jnp.concatenate(lax.all_gather(whole_output, 'dp'), axis=1)  6.3 us
  transfers between devices with their start and end apart: 6, of which 6 were waited for; matrix products, arithmetic and copies ran while one was open for 4% of the time, Pallas kernels for 0%

profile of v1, /device:TPU:0, one launch (start us, length us, event | category | flops | bytes accessed | tf_op | source)
XLA Modules:
  0.0 229.1 jit_solution(6985236189080519574)
XLA Ops:
  6.5 0.7 all-gather.13.cloned.1.call-update
  7.3 0.0 all-gather.7.cloned.1.call-start
  7.3 0.7 all-gather.7.cloned.1.call-update
  8.0 0.0 all-gather.9.cloned.1.call-start
  8.1 0.7 all-gather.9.cloned.1.call-update
  8.7 0.0 all-gather.15.cloned.1.call-start
  8.8 30.9 %all-gather.13.cloned.1.call-done = bf16[1024,512]{1,0:T(8,128)(2,1)} async-done(((bf16[256,512]{1,0:T(8,128)(2,1)}), bf16[1024,512]{1,0:T(8,128)(2,1)}) %all-gather.13.cloned.1.call-update) | async-done | bytes 1048592 | tf_op jit(solution)/shard_map/all_gather | solution.py:51
  39.6 0.0 all-gather.15.cloned.1.call-update
  39.7 0.0 all-gather.11.cloned.1.call-start
  39.7 28.9 %all-gather.7.cloned.1.call-done = bf16[2048,256]{1,0:T(8,128)(2,1)} async-done(((bf16[512,256]{1,0:T(8,128)(2,1)}), bf16[2048,256]{1,0:T(8,128)(2,1)}) %all-gather.7.cloned.1.call-update) | async-done | bytes 1048592 | tf_op jit(solution)/shard_map/all_gather | solution.py:22
  68.6 29.0 %all-gather.9.cloned.1.call-done = bf16[2048,256]{1,0:T(8,128)(2,1)} async-done(((bf16[512,256]{1,0:T(8,128)(2,1)}), bf16[2048,256]{1,0:T(8,128)(2,1)}) %all-gather.9.cloned.1.call-update) | async-done | bytes 1048592 | tf_op jit(solution)/shard_map/all_gather | solution.py:23
  97.6 3.1 %pad_maximum_fusion = bf16[2,2048,256]{2,1,0:T(8,128)(2,1)} fusion(bf16[1,2048,256]{2,1,0:T(8,128)(2,1)} %bitcast.56, bf16[1,2048,256]{2,1,0:T(8,128)(2,1)} %bitcast.55), kind=kLoop, calls=%fused_computation.64 | loop fusion | flops 1048576 | bytes 4194304 | tf_op jit(solution)/shard_map/stack | solution.py:25
  100.6 0.0 all-gather.11.cloned.1.call-update
  100.6 0.9 copy-done.2
  101.6 0.1 fusion.44
  101.6 31.2 %all-gather.15.cloned.1.call-done = bf16[4096,512]{1,0:T(8,128)(2,1)} async-done(((bf16[1024,512]{1,0:T(8,128)(2,1)}), bf16[4096,512]{1,0:T(8,128)(2,1)}) %all-gather.15.cloned.1.call-update) | async-done | bytes 4194320 | tf_op jit(solution)/shard_map/all_gather | solution.py:54
  132.8 6.3 %copy.9 = bf16[1024,4,512]{0,2,1:T(8,128)(2,1)} copy(bf16[1024,4,512]{2,0,1:T(8,128)(2,1)} %bitcast.54) | data formatting | bytes 8388608 | tf_op jit(solution)/shard_map/reshape | solution.py:54
  139.1 54.5 %all-gather.11.cloned.1.call-done = bf16[2,2048,1024]{2,1,0:T(8,128)(2,1)} async-done(((bf16[2,2048,256]{2,1,0:T(8,128)(2,1)}), bf16[2,2048,1024]{2,1,0:T(8,128)(2,1)}) %all-gather.11.cloned.1.call-update) | async-done | bytes 8388624 | tf_op jit(solution)/shard_map/all_gather | solution.py:29
  193.7 8.1 %convert_bitcast_fusion = bf16[2,512,1024]{2,1,0:T(8,128)(2,1)S(1)} fusion(bf16[2,2048,1024]{2,1,0:T(8,128)(2,1)} %all-gather.11.cloned.1.call-done, bf16[1,512,2048]{2,1,0:T(8,128)(2,1)S(1)} %copy-done), kind=kOutput, calls=%fused_computation.68 | convolution fusion | flops 4296015872 | bytes 12582912 | tf_op jit(solution)/shard_map/td,kdc->ktc/dot_general | solution.py:26
  201.7 0.6 multiply_convert_fusion
  202.4 3.4 %collective-permute-start = (bf16[30,1024]{1,0:T(8,128)(2,1)S(1)}, bf16[30,1024]{1,0:T(8,128)(2,1)S(1)}, u32[]{:S(2)}, u32[]{:S(2)}) collective-permute-start(bf16[30,1024]{1,0:T(8,128)(2,1)S(1)} %slice_bitcast_fusion), channel_id=1, source_target_pairs={{0,4},{4,8},{8,12},{1,5},{5,9},{9,13},{2,6},{6,10},{10,14},{3,7},{... | collective-permute-start | bytes 184328 | tf_op jit(solution)/shard_map/ppermute | solution.py:12
  205.8 0.6 fusion.48
  206.4 0.0 copy-start.3
  206.4 1.3 collective-permute-done
  207.7 0.3 maximum_convert_fusion
  208.0 9.7 %fusion.42 = (f32[512]{0:T(512)S(1)}, f32[512,1024]{1,0:T(8,128)S(1)}) fusion(f32[542,1024]{1,0:T(8,128)S(1)} %maximum_convert_fusion, f32[1024]{0:T(1024)S(1)} %bitcast.67, f32[1024]{0:T(1024)S(1)} %bitcast.68, f32[1024]{0:T(1024)S(1)} %bitcast.70, f32[1024]{0:T(1024)S(1)} %bitcast.71, f32[1024]{0:T(1024)S(1)} %bitcast.72, f32[1024]{0:T(1024)S(1)} %bitcast.73, ...), kind=kLoop, calls=%fused_computation.81 | loop fusion | flops 33029632 | bytes 67241984 | tf_op jit(solution)/shard_map/reduce_sum | solution.py:46
  217.7 0.0 copy-start.4
  217.7 0.0 copy-start.5
  217.8 0.3 multiply_reduce_fusion
  218.1 0.3 copy-done.4
  218.4 0.0 copy-done.5
  218.4 4.2 %fusion = bf16[1,512,2048]{2,1,0:T(8,128)(2,1)} fusion(bf16[1024,2048]{0,1:T(8,128)(2,1)S(1)} %bitcast.53, f32[512,1024]{1,0:T(8,128)S(1)} %get-tuple-element.6, f32[1024]{0:T(1024)S(1)} %copy-done.4, f32[1024]{0:T(1024)S(1)} %copy-done.5, f32[512]{0:T(512)S(1)} %add_rsqrt_fusion, f32[512]{0:T(512)S(1)} %broadcast_multiply_fusion), kind=kOutput, calls=%fused_computation.1 | convolution fusion | flops 2153250816 | bytes 8400896 | tf_op jit(solution)/shard_map/dot_general | solution.py:52
  (11 shorter events, 0.1 us)
Async XLA Ops:
  6.5 187.1 %copy-start = (bf16[1,512,2048]{2,1,0:T(8,128)(2,1)S(1)}, bf16[1,512,2048]{2,1,0:T(8,128)(2,1)}, u32[]{:S(2)}) copy-start(bf16[1,512,2048]{2,1,0:T(8,128)(2,1)} %param.8) | copy-start | bytes 6291460
  6.5 33.1 %all-gather.13.cloned.1.call-start = ((), (), s32[]{:S(2)}) async-start(), calls=%async_computation.3 | async-start | bytes 1310720 | tf_op jit(solution)/shard_map/all_gather | solution.py:51
  7.3 61.3 %all-gather.7.cloned.1.call-start = ((), (), s32[]{:S(2)}) async-start(), calls=%async_computation | async-start | bytes 1310720 | tf_op jit(solution)/shard_map/all_gather | solution.py:22
  8.0 89.6 %all-gather.9.cloned.1.call-start = ((), (), s32[]{:S(2)}) async-start(), calls=%async_computation.1 | async-start | bytes 1310720 | tf_op jit(solution)/shard_map/all_gather | solution.py:23
  8.7 124.1 %all-gather.15.cloned.1.call-start = ((), (), s32[]{:S(2)}) async-start(), calls=%async_computation.4 | async-start | bytes 5242880 | tf_op jit(solution)/shard_map/all_gather | solution.py:54
  39.7 154.0 %all-gather.11.cloned.1.call-start = ((), (), s32[]{:S(2)}) async-start(), calls=%async_computation.2 | async-start | bytes 10485760 | tf_op jit(solution)/shard_map/all_gather | solution.py:29
  100.6 0.9 copy-start.2
  202.4 5.3 %collective-permute-start = (bf16[30,1024]{1,0:T(8,128)(2,1)S(1)}, bf16[30,1024]{1,0:T(8,128)(2,1)S(1)}, u32[]{:S(2)}, u32[]{:S(2)}) collective-permute-start(bf16[30,1024]{1,0:T(8,128)(2,1)S(1)} %slice_bitcast_fusion), channel_id=1, source_target_pairs={{0,4},{4,8},{8,12},{1,5},{5,9},{9,13},{2,6},{6,10},{10,14},{3,7},{... | collective-permute-start | bytes 184328 | tf_op jit(solution)/shard_map/ppermute | solution.py:12
  206.4 1.6 copy-start.3
  208.0 10.1 %copy-start.1 = (bf16[1024,4,512]{0,2,1:T(8,128)(2,1)S(1)}, bf16[1024,4,512]{0,2,1:T(8,128)(2,1)}, u32[]{:S(2)}) copy-start(bf16[1024,4,512]{0,2,1:T(8,128)(2,1)} %copy.9) | copy-start | bytes 12582916
  217.7 0.7 copy-start.4
  217.7 0.7 copy-start.5
Sparse Core Ops, SparseCore 0:
  8.9 30.6 all-gather.12
  41.2 27.3 all-gather.6
  70.2 27.3 all-gather.8
  99.0 33.8 all-gather.14
  134.2 59.3 all-gather.10
